TPU v7x, 32 devices: a whole 2x2x4 slice. The times are simulated.
32 devices in a mesh: sp: 32 (over z, y, x, core), tp: 1.
Axes of the slice: x: 2, y: 2, z: 4, core: 2. Of those that a mesh axis runs over, the one named last changes fastest.
Arguments:
- queries: bfloat16 [4096, 2048], P('sp', 'tp'), may hold values from -6 to 6
- forget_logits: bfloat16 [2, 4096, 2048], P(None, 'sp', 'tp'), may hold values from -7.5 to 7.5
- value_matrix: bfloat16 [4096, 2048], P('sp', 'tp'), may hold values from -6 to 6
- output_gate_logits: bfloat16 [4096, 2048], P('sp', 'tp'), may hold values from -6 to 6
- forget_slack: float32 [2048], P('tp'), may hold values from 0.00012207031 to 0.07
- spike_log_forget: float32 [4096, 16], P('sp', 'tp'), may hold values from -2.8 to 0, as said below
- head_norm_gain: bfloat16 [128], replicated, may hold values from 0.099609375 to 1.8984375
- output_weight: bfloat16 [2048, 2048], P('tp'), may hold values from -0.125 to 0.125
- residual: bfloat16 [4096, 2048], P('sp'), may hold values from -6 to 6
- mixer_norm_gain: bfloat16 [2048], replicated, may hold values from 0.099609375 to 1.8984375
- mixer_gate_weight: bfloat16 [2048, 5632], P('sp', 'tp'), may hold values from -0.125 to 0.125
- mixer_up_weight: bfloat16 [2048, 5632], P('sp', 'tp'), may hold values from -0.125 to 0.125
- mixer_down_weight: bfloat16 [5632, 2048], P('tp', 'sp'), may hold values from -0.078125 to 0.078125
Outputs:
- layer_out: bfloat16 [4096, 2048], P(('sp', 'tp'))
Inputs may be any that keep to these rules, and one draw needn't show every extreme that they name: `spike_log_forget`: zero at all but a few tokens.
All inputs are finite; a program needn't handle non-finite values.
Results may differ from a plain program's by a relative error of at most 0.015.
Values may be sent and summed in bfloat16 or wider, within the bound.
A program may use at most 192 MiB of HBM per device.

v0:
```python
import functools

import jax
import jax.numpy as jnp
from jax import lax
from jax.experimental import pallas as pl
from jax.experimental.pallas import tpu as pltpu
from jax.sharding import PartitionSpec as P

NORM_EPS = 1e-06
MESH = pl.DeviceIdType.MESH
PAD_ROWS = 16
GROUP = 8


def dot_nt(a, b):
    return lax.dot_general(a, b, (((1,), (1,)), ((), ())), preferred_element_type=jnp.float32)


def dot_tn(a, b):
    return lax.dot_general(a, b, (((0,), (0,)), ((), ())), preferred_element_type=jnp.float32)


def dot_nn(a, b):
    return jnp.dot(a, b, preferred_element_type=jnp.float32)


def silu(x):
    return x * jax.nn.sigmoid(x)


def split_bf16(x):
    high = x.astype(jnp.bfloat16)
    return high, (x - high.astype(jnp.float32)).astype(jnp.bfloat16)


def sweep_kernel(q_ref, f_ref, v_ref, slack_ref, spike_ref, local_ref, reach_ref, state_ref):
    head = pl.program_id(0)
    rows, width = q_ref.shape
    query = silu(q_ref[...].astype(jnp.float32)) * (width ** -0.5)
    value = v_ref[...]
    spikes = spike_ref[...]
    lane = lax.broadcasted_iota(jnp.int32, spikes.shape, 1)
    spike = jnp.sum(jnp.where(lane == head, spikes, 0.0), axis=1, keepdims=True)
    slack = slack_ref[...]
    down = lax.broadcasted_iota(jnp.int32, (rows, rows), 0)
    across = lax.broadcasted_iota(jnp.int32, (rows, rows), 1)
    scores = None
    for way in (0, 1):
        mask = (down >= across) if way == 0 else (down <= across)
        tri = jnp.where(mask, 1.0, 0.0).astype(jnp.bfloat16)
        key = slack * jax.nn.sigmoid(-f_ref[way].astype(jnp.float32))
        decay = jnp.log1p(-key) + spike
        high, low = split_bf16(decay)
        running = dot_nn(tri, high) + dot_nn(tri, low)
        final = running[rows - 1 : rows] if way == 0 else running[0:1]
        query_scaled = (query * jnp.exp(running)).astype(jnp.bfloat16)
        key_scaled = (key * jnp.exp(-running)).astype(jnp.bfloat16)
        key_end = (key * jnp.exp(final - running)).astype(jnp.bfloat16)
        part = jnp.where(mask, dot_nt(query_scaled, key_scaled), 0.0)
        scores = part if scores is None else scores + part
        reach_ref[way] = query_scaled
        state_ref[way, 0, 0:width] = dot_tn(value, key_end).astype(jnp.bfloat16)
        total_high, total_low = split_bf16(jnp.exp(final))
        place = lax.broadcasted_iota(jnp.int32, (PAD_ROWS, width), 0)
        state_ref[way, 0, width : width + PAD_ROWS] = jnp.where(
            place == 0,
            total_high.astype(jnp.float32),
            jnp.where(place == 1, total_low.astype(jnp.float32), 0.0),
        ).astype(jnp.bfloat16)
    local_ref[...] = dot_nn(scores.astype(jnp.bfloat16), value)


def sweep(queries, forget_logits, values, slack, spike):
    rows, columns = queries.shape
    heads = spike.shape[1]
    width = columns // heads
    by_head = pl.BlockSpec((rows, width), lambda h: (0, h))
    return pl.pallas_call(
        sweep_kernel,
        grid=(heads,),
        in_specs=[
            by_head,
            pl.BlockSpec((2, rows, width), lambda h: (0, 0, h)),
            by_head,
            pl.BlockSpec((1, width), lambda h: (0, h)),
            pl.BlockSpec((rows, heads), lambda h: (0, 0)),
        ],
        out_specs=[
            by_head,
            pl.BlockSpec((2, rows, width), lambda h: (0, 0, h)),
            pl.BlockSpec((2, 1, width + PAD_ROWS, width), lambda h: (0, h, 0, 0)),
        ],
        out_shape=[
            jax.ShapeDtypeStruct((rows, columns), jnp.float32),
            jax.ShapeDtypeStruct((2, rows, columns), jnp.bfloat16),
            jax.ShapeDtypeStruct((2, heads, width + PAD_ROWS, width), jnp.bfloat16),
        ],
        cost_estimate=pl.CostEstimate(
            flops=20 * rows * width * columns, bytes_accessed=8 * rows * columns, transcendentals=8 * rows * columns
        ),
        name="sweep",
    )(queries, forget_logits, values, slack.reshape(1, columns), spike)


def greet(axis, others, count):
    barrier = pltpu.get_barrier_semaphore()

    def signal(k, carry):
        pl.semaphore_signal(barrier, inc=1, device_id={axis: others(k)}, device_id_type=MESH)
        return carry

    lax.fori_loop(1, count, signal, 0)
    pl.semaphore_wait(barrier, count - 1)


def exchange_kernel(n, state_ref, enter_ref, held, made, out_sem, in_sem, out_sem2, in_sem2):
    me = lax.axis_index("sp")
    rows = enter_ref.shape[1]

    def other(k):
        return lax.rem(me + k, n)

    greet("sp", other, n)

    def first(k):
        there = other(k)
        return pltpu.make_async_remote_copy(
            src_ref=state_ref.at[there],
            dst_ref=held.at[me],
            send_sem=out_sem.at[k],
            recv_sem=in_sem.at[k],
            device_id={"sp": there},
            device_id_type=MESH,
        )

    def second(k):
        there = other(k)
        return pltpu.make_async_remote_copy(
            src_ref=made.at[there],
            dst_ref=enter_ref.at[me],
            send_sem=out_sem2.at[k],
            recv_sem=in_sem2.at[k],
            device_id={"sp": there},
            device_id_type=MESH,
        )

    def go(copy):
        def start(k, carry):
            copy(k).start()
            return carry

        lax.fori_loop(1, n, start, 0)

    def end(copy):
        def wait(k, carry):
            copy(k).wait()
            return carry

        lax.fori_loop(1, n, wait, 0)

    go(first)
    held[me] = state_ref[me]
    end(first)
    backward = me // (n // 2)

    def step(i, total):
        source = i + backward * (n - 1 - 2 * i)
        made[source] = total.astype(jnp.bfloat16)
        block = held[source].astype(jnp.float32)
        factor = block[rows : rows + 1] + block[rows + 1 : rows + 2]
        return factor * total + block[:rows]

    lax.fori_loop(0, n, step, jnp.zeros(enter_ref.shape[1:], jnp.float32))
    go(second)
    enter_ref[me] = made[me]
    end(second)


def exchange(states):
    n = lax.axis_size("sp")
    ways, heads, padded, width = states.shape
    depth = padded - PAD_ROWS
    cuts = n // (ways * heads)
    rows = depth // cuts
    if cuts > 1:
        body = states[:, :, :depth].reshape(ways, heads, cuts, rows, width)
        tail = jnp.broadcast_to(
            states[:, :, None, depth:], (ways, heads, cuts, PAD_ROWS, width)
        )
        states = jnp.concatenate([body, tail], axis=3)
    entered = pl.pallas_call(
        functools.partial(exchange_kernel, n),
        in_specs=[pl.BlockSpec(memory_space=pltpu.VMEM)],
        out_specs=pl.BlockSpec(memory_space=pltpu.VMEM),
        out_shape=jax.ShapeDtypeStruct((n, rows, width), jnp.bfloat16),
        scratch_shapes=[
            pltpu.VMEM((n, rows + PAD_ROWS, width), jnp.bfloat16),
            pltpu.VMEM((n, rows, width), jnp.bfloat16),
            pltpu.SemaphoreType.DMA((n,)),
            pltpu.SemaphoreType.DMA((n,)),
            pltpu.SemaphoreType.DMA((n,)),
            pltpu.SemaphoreType.DMA((n,)),
        ],
        compiler_params=pltpu.CompilerParams(collective_id=1, has_side_effects=True),
        name="exchange",
    )(states.reshape(n, rows + PAD_ROWS, width))
    return entered.reshape(ways, heads, depth, width)


def reshard_kernel(g, *refs):
    count = (len(refs) - 3) // 2
    gives, takes = refs[:count], refs[count : 2 * count]
    out_sem, in_sem, own_sem = refs[2 * count :]
    me = lax.axis_index("sp")
    base = me // g * g
    seat = me - base

    def other(k):
        return lax.rem(seat + k, g)

    greet("sp", lambda k: base + other(k), g)
    copies = []
    for k in range(1, g):
        there = other(k)
        for i in range(count):
            copies.append(
                pltpu.make_async_remote_copy(
                    src_ref=gives[i].at[there],
                    dst_ref=takes[i].at[seat],
                    send_sem=out_sem.at[i, k],
                    recv_sem=in_sem.at[i, k],
                    device_id={"sp": base + there},
                    device_id_type=MESH,
                )
            )
            copies[-1].start()
    for i in range(count):
        copies.append(pltpu.make_async_copy(gives[i].at[seat], takes[i].at[seat], own_sem.at[i]))
        copies[-1].start()
    for copy in copies:
        copy.wait()


def reshard(arrays, g, collective_id):
    count = len(arrays)
    return pl.pallas_call(
        functools.partial(reshard_kernel, g),
        in_specs=[pl.BlockSpec(memory_space=pltpu.VMEM)] * count,
        out_specs=[pl.BlockSpec(memory_space=pltpu.VMEM)] * count,
        out_shape=[jax.ShapeDtypeStruct(a.shape, a.dtype) for a in arrays],
        scratch_shapes=[
            pltpu.SemaphoreType.DMA((count, g)),
            pltpu.SemaphoreType.DMA((count, g)),
            pltpu.SemaphoreType.DMA((count,)),
        ],
        compiler_params=pltpu.CompilerParams(
            collective_id=collective_id, has_side_effects=True
        ),
        name="reshard",
    )(*arrays)


def gather_kernel(g, give, take, out_sem, in_sem):
    me = lax.axis_index("sp")
    base = me // g * g
    seat = me - base

    def other(k):
        return lax.rem(seat + k, g)

    greet("sp", lambda k: base + other(k), g)
    copies = []
    for k in range(1, g):
        copies.append(
            pltpu.make_async_remote_copy(
                src_ref=give,
                dst_ref=take.at[seat],
                send_sem=out_sem.at[k],
                recv_sem=in_sem.at[k],
                device_id={"sp": base + other(k)},
                device_id_type=MESH,
            )
        )
        copies[-1].start()
    take[seat] = give[...]
    for copy in copies:
        copy.wait()


def gather(array, g, collective_id):
    return pl.pallas_call(
        functools.partial(gather_kernel, g),
        in_specs=[pl.BlockSpec(memory_space=pltpu.VMEM)],
        out_specs=pl.BlockSpec(memory_space=pltpu.VMEM),
        out_shape=jax.ShapeDtypeStruct((g,) + array.shape, array.dtype),
        scratch_shapes=[pltpu.SemaphoreType.DMA((g,)), pltpu.SemaphoreType.DMA((g,))],
        compiler_params=pltpu.CompilerParams(
            collective_id=collective_id, has_side_effects=True
        ),
        name="gather",
    )(array).reshape((g * array.shape[0],) + array.shape[1:])


def project_kernel(local_ref, reach_ref, enter_ref, gain_ref, gate_ref, weight_ref, out_ref, total):
    head = pl.program_id(0)
    mix = (
        local_ref[...]
        + dot_nt(reach_ref[0], enter_ref[0, 0])
        + dot_nt(reach_ref[1], enter_ref[1, 0])
    )
    scale = lax.rsqrt(jnp.mean(mix * mix, axis=-1, keepdims=True) + NORM_EPS)
    gate = silu(gate_ref[...].astype(jnp.float32))
    mixed = (mix * scale * gain_ref[...].astype(jnp.float32) * gate).astype(jnp.bfloat16)
    term = dot_nn(mixed, weight_ref[...])

    @pl.when(head == 0)
    def _():
        total[...] = term

    @pl.when(head > 0)
    def _():
        total[...] += term

    @pl.when(head == pl.num_programs(0) - 1)
    def _():
        out_ref[...] = total[...].astype(jnp.bfloat16)


def project(local, reach, entered, gain, gate_logits, weight):
    rows, columns = local.shape
    heads, width = entered.shape[1], entered.shape[3]
    model = weight.shape[1]
    by_head = pl.BlockSpec((rows, width), lambda h: (0, h))
    return pl.pallas_call(
        project_kernel,
        grid=(heads,),
        in_specs=[
            by_head,
            pl.BlockSpec((2, rows, width), lambda h: (0, 0, h)),
            pl.BlockSpec((2, 1, width, width), lambda h: (0, h, 0, 0)),
            pl.BlockSpec((1, width), lambda h: (0, 0)),
            by_head,
            pl.BlockSpec((width, model), lambda h: (h, 0)),
        ],
        out_specs=pl.BlockSpec((rows, model), lambda h: (0, 0)),
        out_shape=jax.ShapeDtypeStruct((rows, model), jnp.bfloat16),
        scratch_shapes=[pltpu.VMEM((rows, model), jnp.float32)],
        cost_estimate=pl.CostEstimate(
            flops=2 * rows * columns * model, bytes_accessed=2 * columns * model, transcendentals=rows * columns
        ),
        name="project",
    )(local, reach, entered, gain.reshape(1, width), gate_logits, weight)


def local(
    queries,
    forget_logits,
    value_matrix,
    output_gate_logits,
    forget_slack,
    spike_log_forget,
    head_norm_gain,
    output_weight,
    residual,
    mixer_norm_gain,
    mixer_gate_weight,
    mixer_up_weight,
    mixer_down_weight,
):
    n, tp = lax.axis_size("sp"), lax.axis_size("tp")
    g = GROUP
    row_count = queries.shape[0]
    depth, units = mixer_gate_weight.shape
    far = [[b * g + j for b in range(n // g)] for j in range(g)]

    def cut(weight):
        return weight.reshape(depth, g, units // g).transpose(1, 0, 2)

    pieces = reshard([cut(mixer_gate_weight), cut(mixer_up_weight), cut(mixer_down_weight.T)], g, 2)
    gate_weight, up_weight, down_weight = (
        lax.all_gather(
            p.reshape(g * depth, units // g), "sp", axis=0, tiled=True, axis_index_groups=far
        )
        for p in pieces
    )

    local_out, reach, states = sweep(
        queries, forget_logits, value_matrix, forget_slack, spike_log_forget
    )
    entered = exchange(states)
    part = project(local_out, reach, entered, head_norm_gain, output_gate_logits, output_weight)
    part_rows = row_count // tp
    if tp > 1:
        part = lax.psum_scatter(part, "tp", scatter_dimension=0, tiled=True)
        residual = lax.dynamic_slice_in_dim(
            residual, lax.axis_index("tp") * part_rows, part_rows, 0
        )
    hidden = (residual.astype(jnp.float32) + part.astype(jnp.float32)).astype(jnp.bfloat16)
    hidden_f = hidden.astype(jnp.float32)
    normed = (
        hidden_f
        * lax.rsqrt(jnp.mean(hidden_f * hidden_f, axis=-1, keepdims=True) + NORM_EPS)
        * mixer_norm_gain.astype(jnp.float32)
    ).astype(jnp.bfloat16)
    normed = gather(normed, g, 4)
    if tp > 1:
        normed = lax.all_gather(normed, "tp", axis=0, tiled=True)
    gate_act = dot_nn(normed, gate_weight)
    up_act = dot_nn(normed, up_weight)
    inner = (silu(gate_act) * up_act).astype(jnp.bfloat16)
    lowered = dot_nt(inner, down_weight).astype(jnp.bfloat16)
    if tp > 1:
        lowered = lax.psum_scatter(lowered, "tp", scatter_dimension=0, tiled=True)
    (terms,) = reshard([lowered.reshape(g, part_rows, lowered.shape[1])], g, 3)
    added = jnp.sum(terms.astype(jnp.float32), axis=0)
    return (hidden_f + added).astype(jnp.bfloat16)


def solution(mesh):
    placed = (
        P("sp", "tp"),
        P(None, "sp", "tp"),
        P("sp", "tp"),
        P("sp", "tp"),
        P("tp"),
        P("sp", "tp"),
        P(),
        P("tp", None),
        P("sp", None),
        P(),
        P("sp", "tp"),
        P("sp", "tp"),
        P("tp", "sp"),
    )
    return jax.shard_map(
        local, mesh=mesh, in_specs=placed, out_specs=P(("sp", "tp"), None), check_vma=False
    )
```

profile of v0, /device:TPU:8, one launch (start us, length us, event | category | flops | bytes accessed | tf_op | source)
XLA Modules:
  0.0 353.0 jit_solution(7320738690922416834)
XLA Ops:
  6.5 0.0 copy-start.2
  6.5 0.0 copy-start.3
  6.5 0.0 all-gather.4.cloned.1.call-start
  6.5 2.0 reshape.50
  8.5 1.0 copy.22
  9.5 0.0 copy-done.2
  9.5 0.7 reshape.51
  10.2 0.0 copy-done.3
  10.2 0.7 reshape.52
  10.9 1.5 copy_bitcast_fusion
  12.4 0.0 copy-start.5
  12.4 0.0 copy-start.4
  12.4 31.8 %reshard.2 = (bf16[8,64,704]{2,1,0:T(8,128)(2,1)}, bf16[8,64,704]{2,1,0:T(8,128)(2,1)}, bf16[8,64,704]{2,1,0:T(8,128)(2,1)}) custom-call(bf16[8,64,704]{2,1,0:T(8,128)(2,1)} %bitcast.26, bf16[8,64,704]{2,1,0:T(8,128)(2,1)} %get-tuple-element.18.refs_1_, bf16[8,64,704]{2,1,0:T(8,128)(2,1)} %get-tuple-element.17.refs_2_), custom_call_target="tpu_custom_call" | custom-call | tf_op jit(solution)/shard_map/reshard/pallas_call | solution.py:247
  44.2 0.0 all-gather.4.cloned.1.call-update
  44.2 0.0 all-gather.6.cloned.1.call-start
  44.3 0.7 all-gather.6.cloned.1.call-update
  45.0 0.0 all-gather.8.cloned.1.call-start
  45.0 0.7 all-gather.8.cloned.1.call-update
  45.7 0.0 copy-done.5
  45.7 0.0 copy-done.4
  45.8 0.7 copy.15.spike_ref
  46.5 14.8 %sweep.1 = (f32[128,2048]{1,0:T(8,128)}, bf16[2,128,2048]{2,1,0:T(8,128)(2,1)}, bf16[2,16,144,128]{3,2,1,0:T(8,128)(2,1)}) custom-call(bf16[128,2048]{1,0:T(8,128)(2,1)} %q_ref.1, bf16[2,128,2048]{2,1,0:T(8,128)(2,1)} %f_ref.1, bf16[128,2048]{1,0:T(8,128)(2,1)} %v_ref.1, f32[1,2048]{1,0:T(1,128)} %bitcast.33, f32[128,16]{1,0:T(8,128)} %copy.15.spike_ref), custom_call_target="tpu_custom_call" | custom-call | flops 671088640 | bytes 2097152 | tf_op jit(solution)/shard_map/sweep/pallas_call | solution.py:79
  61.3 93.7 %exchange.1 = bf16[32,128,128]{2,1,0:T(8,128)(2,1)} custom-call(bf16[32,144,128]{2,1,0:T(8,128)(2,1)} %bitcast.27), custom_call_target="tpu_custom_call" | custom-call | tf_op jit(solution)/shard_map/exchange/pallas_call | solution.py:192
  155.0 0.0 copy-start.1
  155.0 16.7 %project.1 = bf16[128,2048]{1,0:T(8,128)(2,1)} custom-call(f32[128,2048]{1,0:T(8,128)} %get-tuple-element.11.local_ref, bf16[2,128,2048]{2,1,0:T(8,128)(2,1)} %get-tuple-element.12.reach_ref, bf16[2,16,128,128]{3,2,1,0:T(8,128)(2,1)} %bitcast.22, bf16[1,128]{1,0:T(2,128)(2,1)} %bitcast.32, bf16[128,2048]{1,0:T(8,128)(2,1)} %gate_ref.1, ...), custom_call_target="tpu_custom_call" | custom-call | flops 1073741824 | bytes 8388608 | tf_op jit(solution)/shard_map/project/pallas_call | solution.py:335
  171.7 0.0 copy-done.1
  171.7 1.3 fusion
  173.0 2.0 fusion.2.give
  175.1 54.4 %gather.1 = bf16[8,128,2048]{2,1,0:T(8,128)(2,1)} custom-call(bf16[128,2048]{1,0:T(8,128)(2,1)} %fusion.2.give), custom_call_target="tpu_custom_call" | custom-call | tf_op jit(solution)/shard_map/gather/pallas_call | solution.py:292
  229.5 0.0 all-gather.4.cloned.1.call-done
  229.5 6.0 %fusion.5 = f32[1024,704]{0,1:T(8,128)S(1)} fusion(bf16[1024,2048]{1,0:T(8,128)(2,1)} %bitcast.23, bf16[2048,704]{1,0:T(8,128)(2,1)} %all-gather.4.cloned.1.call-done), kind=kOutput, calls=%fused_computation.16 | convolution fusion | flops 2952790016 | bytes 9961472 | tf_op jit(solution)/shard_map/dot_general | solution.py:25
  235.5 0.0 all-gather.6.cloned.1.call-done
  235.5 42.8 %all-gather.8.cloned.1.call-done = bf16[2048,704]{1,0:T(8,128)(2,1)} async-done(((bf16[512,704]{1,0:T(8,128)(2,1)}), bf16[2048,704]{1,0:T(8,128)(2,1)}) %all-gather.8.cloned.1.call-update) | async-done | bytes 2883600 | tf_op jit(solution)/shard_map/all_gather | solution.py:382
  278.3 11.9 %convolution_convert_fusion = bf16[1024,2048]{1,0:T(8,128)(2,1)} fusion(bf16[2048,704]{1,0:T(8,128)(2,1)} %all-gather.8.cloned.1.call-done, f32[1024,704]{0,1:T(8,128)S(1)} %fusion.5, bf16[1024,2048]{1,0:T(8,128)(2,1)} %bitcast.24, bf16[2048,704]{1,0:T(8,128)(2,1)} %all-gather.6.cloned.1.call-done), kind=kOutput, calls=%fused_computation.1 | convolution fusion | flops 5912002560 | bytes 17039360 | tf_op jit(solution)/shard_map/dot_general | solution.py:17
  290.2 52.2 %reshard.3 = bf16[8,128,2048]{2,1,0:T(8,128)(2,1)} custom-call(bf16[8,128,2048]{2,1,0:T(8,128)(2,1)} %bitcast.25), custom_call_target="tpu_custom_call" | custom-call | tf_op jit(solution)/shard_map/reshard/pallas_call | solution.py:247
  342.4 0.0 copy-start
  342.4 3.0 convert_reduce_fusion
  345.4 0.0 copy-done
  345.4 1.0 fusion.3
  (2 shorter events, 0.0 us)
Async XLA Ops:
  6.5 3.0 copy-start.2
  6.5 3.7 %copy-start.3 = (bf16[5632,64]{0,1:T(8,128)(2,1)S(1)}, bf16[5632,64]{0,1:T(8,128)(2,1)}, u32[]{:S(2)}) copy-start(bf16[5632,64]{0,1:T(8,128)(2,1)} %param.25) | copy-start | bytes 2162692
  6.5 223.0 %all-gather.4.cloned.1.call-start = ((), (), s32[]{:S(2)}) async-start(), calls=%async_computation | async-start | bytes 3932160 | tf_op jit(solution)/shard_map/all_gather | solution.py:382
  12.4 33.3 %copy-start.5 = (bf16[2048]{0:T(1024)(128)(2,1)S(1)}, bf16[2048]{0:T(1024)(128)(2,1)}, u32[]{:S(2)}) copy-start(bf16[2048]{0:T(1024)(128)(2,1)} %param.22) | copy-start | bytes 12292
  12.4 33.4 %copy-start.4 = (f32[128,16]{0,1:T(8,128)S(1)}, f32[128,16]{0,1:T(8,128)}, u32[]{:S(2)}) copy-start(f32[128,16]{0,1:T(8,128)} %param.18) | copy-start | bytes 24580
  44.2 191.3 %all-gather.6.cloned.1.call-start = ((), (), s32[]{:S(2)}) async-start(), calls=%async_computation.1 | async-start | bytes 3932160 | tf_op jit(solution)/shard_map/all_gather | solution.py:382
  45.0 233.3 %all-gather.8.cloned.1.call-start = ((), (), s32[]{:S(2)}) async-start(), calls=%async_computation.2 | async-start | bytes 3932160 | tf_op jit(solution)/shard_map/all_gather | solution.py:382
  155.0 16.7 %copy-start.1 = (bf16[128,2048]{1,0:T(8,128)(2,1)S(1)}, bf16[128,2048]{1,0:T(8,128)(2,1)}, u32[]{:S(2)}) copy-start(bf16[128,2048]{1,0:T(8,128)(2,1)} %param.21) | copy-start | bytes 1572868
  342.4 3.1 copy-start
Sparse Core Ops, SparseCore 0:
  44.4 103.0 all-gather.3
  149.0 65.5 all-gather.5
  216.2 62.0 all-gather.7
where the time goes:
time: 359 us; the launch traced here: 353 us
  Pallas kernels  264 us (74%)
  waiting for transfers between devices  44.2 us (12%)
  matrix products  17.9 us (5%)
  between operations  13.3 us (4%)
  other arithmetic  7.38 us (2%)
  local copies, waits for them, and re-layouts  6.58 us (2%)
    pallas_call x1, Pallas kernels, exchange(): pl.pallas_call(functools.partial(exchange_kernel, n), in_specs=[pl.BlockS...  93.7 us
    pallas_call x2, Pallas kernels, reshard(): pl.pallas_call(functools.partial(reshard_kernel, g), in_specs=[pl.BlockSp...  84 us
    pallas_call x1, Pallas kernels, gather(): pl.pallas_call(functools.partial(gather_kernel, g), in_specs=[pl.BlockSpe...  54.4 us
    all_gather x3, waiting for transfers between devices, local(): lax.all_gather(p.reshape(g * depth, units // g), 'sp', axis=0, tiled=True...  42.8 us
    pallas_call x1, Pallas kernels, project(): pl.pallas_call(project_kernel, grid=(heads,), in_specs=[by_head, pl.Block...  16.7 us
    pallas_call x1, Pallas kernels, sweep(): pl.pallas_call(sweep_kernel, grid=(heads,), in_specs=[by_head, pl.BlockSp...  14.8 us
    dot_general x1, matrix products, dot_nt(): lax.dot_general(a, b, (((1,), (1,)), ((), ())), preferred_element_type=jn...  11.9 us
  transfers between devices with their start and end apart: 3, of which 1 were waited for; matrix products, arithmetic and copies ran while one was open for 3% of the time, Pallas kernels for 51%

commit v1 on v0

--- a/solution.py
+++ b/solution.py
@@ -353,6 +353,487 @@
     )(local, reach, entered, gain.reshape(1, width), gate_logits, weight)
 
 
+CORES = 2
+PLANE = 4
+
+
+def flip(i, k):
+    out, bit = i, 1
+    while bit <= k:
+        if k & bit:
+            out = out + bit - 2 * bit * (lax.rem(i // bit, 2))
+        bit *= 2
+    return out
+
+
+def layer_kernel(
+    nz,
+    q_hbm, f_hbm, v_hbm, og_hbm, res_hbm, slack_ref, spike_ref, hgain_ref, mgain_ref, wo_hbm, gate_hbm, up_hbm, down_hbm,
+    out_ref,
+    q_v, f_v, v_v, og_v, res_v, wo_v, w_v,
+    reach, scaled, locals_, states, held, total, totals_in, entry, made, enter, mixed, tok, parts, terms,
+    in_sem, w0_sem, w1_out, w1_in, x_out, x_in, y_out, y_in, d_out, d_in, p_out, p_in,
+    s1_out, s1_in, s2_out, s2_in, s3_out, s3_in, up_out, up_in, dn_out, dn_in, r_out, r_in,
+):
+    rows, columns = q_v.shape
+    width = hgain_ref.shape[1]
+    heads = columns // width
+    depth = gate_hbm.shape[0]
+    units = w_v.shape[2]
+    side = PLANE * CORES
+    per = 2 * heads // side
+    half = side // 2
+    me = lax.axis_index("sp")
+    z, seat = me // side, lax.rem(me, side)
+    q, c = seat // CORES, lax.rem(seat, CORES)
+    base = z * side
+
+    def at(zz, qq, cc):
+        return zz * side + qq * CORES + cc
+
+    def copy(src, dst, out_sem, got_sem, there):
+        return pltpu.make_async_remote_copy(
+            src_ref=src, dst_ref=dst, send_sem=out_sem, recv_sem=got_sem,
+            device_id={"sp": there}, device_id_type=MESH,
+        )
+
+    zs = [z] + [flip(z, k) for k in range(1, nz)]
+    qs = [q] + [flip(q, k) for k in range(1, PLANE)]
+    along = [at(zz, q, c) for zz in zs]
+    x_dev, y_dev, p_dev = at(z, qs[1], c), at(z, qs[2], c), at(z, q, 1 - c)
+
+    loads = [
+        pltpu.make_async_copy(src, dst, in_sem.at[i])
+        for i, (src, dst) in enumerate(
+            ((f_hbm, f_v), (q_hbm, q_v), (v_hbm, v_v), (og_hbm, og_v), (res_hbm, res_v), (wo_hbm, wo_v))
+        )
+    ]
+    weights = (gate_hbm, up_hbm, down_hbm)
+
+    def cut(a, zz):
+        return weights[a].at[:, pl.ds(pl.multiple_of(zz * units, 128), units)]
+
+    def piece(zz, qq, cc):
+        return w_v.at[:, pl.ds(pl.multiple_of(at(zz, qq, cc) * depth, depth), depth), :]
+
+    def strip(a, device):
+        return w_v.at[a, pl.ds(pl.multiple_of(device * depth, depth), depth), :]
+
+    own = [pltpu.make_async_copy(cut(a, z), strip(a, me), w0_sem.at[a]) for a in range(3)]
+    for load in loads[:3]:
+        load.start()
+    for load in own:
+        load.start()
+
+    barrier = pltpu.get_barrier_semaphore()
+    for k in range(1, nz):
+        pl.semaphore_signal(barrier, inc=1, device_id={"sp": along[k]}, device_id_type=MESH)
+    for k in range(1, side):
+        pl.semaphore_signal(
+            barrier, inc=1, device_id={"sp": base + lax.rem(seat + k, side)}, device_id_type=MESH
+        )
+    pl.semaphore_wait(barrier, nz - 1 + side - 1)
+
+    def first(k):
+        return [copy(cut(a, zs[k]), strip(a, me), w1_out.at[a, k], w1_in.at[a, k], along[k]) for a in range(3)]
+
+    def plane(k, sems, there):
+        src = piece(zs[k], q, c)
+        return copy(src, src, sems[0].at[k], sems[1].at[k], there)
+
+    def corner(k):
+        near, there = (1, y_dev) if k < nz // 2 else (2, x_dev)
+        src = piece(zs[k], qs[near], c)
+        return copy(src, src, d_out.at[k], d_in.at[k], there)
+
+    def partner(k, j):
+        src = piece(zs[k], qs[j], c)
+        return copy(src, src, p_out.at[k, j], p_in.at[k, j], p_dev)
+
+    def spread(k):
+        if k == 0:
+            for load in own:
+                load.wait()
+        else:
+            for one in first(k):
+                one.wait_recv()
+        plane(k, (x_out, x_in), x_dev).start()
+        plane(k, (y_out, y_in), y_dev).start()
+        partner(k, 0).start()
+
+    def onward(k):
+        plane(k, (x_out, x_in), x_dev).wait_recv()
+        if k < nz // 2:
+            corner(k).start()
+        partner(k, 1).start()
+        plane(k, (y_out, y_in), y_dev).wait_recv()
+        if k >= nz // 2:
+            corner(k).start()
+        partner(k, 2).start()
+
+    def last(k):
+        corner(k).wait_recv()
+        partner(k, 3).start()
+
+    late = nz - 1
+    for k in range(1, late):
+        for one in first(k):
+            one.start()
+    spread(0)
+    for load in loads[3:]:
+        load.start()
+
+    down = lax.broadcasted_iota(jnp.int32, (rows, rows), 0)
+    across = lax.broadcasted_iota(jnp.int32, (rows, rows), 1)
+    masks = (down >= across, down <= across)
+    for load in loads[:3]:
+        load.wait()
+    spikes = spike_ref[...]
+    lane = lax.broadcasted_iota(jnp.int32, spikes.shape, 1)
+    place = lax.broadcasted_iota(jnp.int32, (PAD_ROWS, width), 0)
+
+    def pad(decay):
+        high, low = split_bf16(decay)
+        return jnp.where(
+            place == 0, high.astype(jnp.float32), jnp.where(place == 1, low.astype(jnp.float32), 0.0)
+        ).astype(jnp.bfloat16)
+
+    def by_head(head):
+        return pl.ds(pl.multiple_of(head * width, width), width)
+
+    def state_copy(w):
+        return copy(states.at[w], held.at[seat], s1_out.at[w], s1_in.at[seat], base + w)
+
+    def state_arrival(w):
+        return copy(states.at[w], held.at[w], s1_out.at[w], s1_in.at[w], base + w)
+
+    def make_states(group):
+        def step(i, carry):
+            head = group * per + i
+            lanes = by_head(head)
+            query = silu(q_v[:, lanes].astype(jnp.float32)) * (width ** -0.5)
+            value = v_v[:, lanes]
+            spike = jnp.sum(jnp.where(lane == head, spikes, 0.0), axis=1, keepdims=True)
+            slack = slack_ref[:, lanes]
+            for way in (0, 1):
+                tri = jnp.where(masks[way], 1.0, 0.0).astype(jnp.bfloat16)
+                key = slack * jax.nn.sigmoid(-f_v[way, :, lanes].astype(jnp.float32))
+                decay = jnp.log1p(-key) + spike
+                high, low = split_bf16(decay)
+                running = dot_nn(tri, high) + dot_nn(tri, low)
+                final = running[rows - 1 : rows] if way == 0 else running[0:1]
+                reach[way, :, lanes] = (query * jnp.exp(running)).astype(jnp.bfloat16)
+                scaled[way, :, lanes] = (key * jnp.exp(-running)).astype(jnp.bfloat16)
+                key_end = (key * jnp.exp(final - running)).astype(jnp.bfloat16)
+                states[way * half + group, i, 0:width] = dot_tn(value, key_end).astype(jnp.bfloat16)
+                states[way * half + group, i, width : width + PAD_ROWS] = pad(jnp.exp(final))
+            return carry
+
+        lax.fori_loop(0, per, step, 0)
+
+    for group in range(half):
+        make_states(group)
+        for w in (group, half + group):
+            @pl.when(w != seat)
+            def _(w=w):
+                state_copy(w).start()
+
+            @pl.when(w == seat)
+            def _(w=w):
+                held[w] = states[w]
+
+    def local_step(head, carry):
+        lanes = by_head(head)
+        scores = None
+        for way in (0, 1):
+            part = jnp.where(masks[way], dot_nt(reach[way, :, lanes], scaled[way, :, lanes]), 0.0)
+            scores = part if scores is None else scores + part
+        locals_[:, lanes] = dot_nn(scores.astype(jnp.bfloat16), v_v[:, lanes])
+        return carry
+
+    lax.fori_loop(0, heads, local_step, 0)
+
+    spread(1)
+    onward(0)
+
+    for w in range(side):
+        @pl.when(w != seat)
+        def _(w=w):
+            state_arrival(w).wait_recv()
+
+    back = seat // half
+
+    def turn(i, count):
+        return i + back * (count - 1 - 2 * i)
+
+    def unpack(block):
+        return block[:, width : width + 1] + block[:, width + 1 : width + 2], block[:, :width]
+
+    entry[...] = jnp.zeros_like(entry)
+
+    def first_pass(i, decay):
+        factor, state = unpack(held[turn(i, side)].astype(jnp.float32))
+        entry[...] = factor * entry[...] + state
+        return factor * decay
+
+    decay = lax.fori_loop(0, side, first_pass, jnp.ones((per, 1, width), jnp.float32))
+    total[:, 0:width] = entry[...].astype(jnp.bfloat16)
+    for i in range(per):
+        total[i, width : width + PAD_ROWS] = pad(decay[i])
+
+    def give_after(k):
+        return (zs[k] > z) == (back == 0)
+
+    def total_copy(k):
+        return copy(total, totals_in.at[z], s2_out.at[k], s2_in.at[k], along[k])
+
+    for k in range(1, nz):
+        @pl.when(give_after(k))
+        def _(k=k):
+            total_copy(k).start()
+    for one in first(late):
+        one.start()
+    entry[...] = jnp.zeros_like(entry)
+    for k in range(1, nz):
+        @pl.when(jnp.logical_not(give_after(k)))
+        def _(k=k):
+            total_copy(k).wait_recv()
+    for i in range(nz):
+        source = turn(i, nz)
+
+        @pl.when(jnp.logical_and(source != z, (source < z) == (back == 0)))
+        def _(source=source):
+            factor, state = unpack(totals_in[source].astype(jnp.float32))
+            entry[...] = factor * entry[...] + state
+
+    def enter_copy(w):
+        return copy(made.at[w], enter.at[seat], s3_out.at[w], s3_in.at[seat], base + w)
+
+    def enter_arrival(w):
+        return copy(made.at[w], enter.at[w], s3_out.at[w], s3_in.at[w], base + w)
+
+    def second_pass(i, carry):
+        source = turn(i, side)
+        made[source] = entry[...].astype(jnp.bfloat16)
+
+        @pl.when(source != seat)
+        def _():
+            enter_copy(source).start()
+
+        factor, state = unpack(held[source].astype(jnp.float32))
+        entry[...] = factor * entry[...] + state
+        return carry
+
+    lax.fori_loop(0, side, second_pass, 0)
+    enter[seat] = made[seat]
+
+    spread(2)
+    onward(1)
+    last(0)
+    for load in loads[3:]:
+        load.wait()
+    for w in range(side):
+        @pl.when(w != seat)
+        def _(w=w):
+            enter_arrival(w).wait_recv()
+
+    def mix_step(head, carry):
+        lanes = by_head(head)
+        group, i = head // per, lax.rem(head, per)
+        mix = (
+            locals_[:, lanes]
+            + dot_nt(reach[0, :, lanes], enter[group, i])
+            + dot_nt(reach[1, :, lanes], enter[half + group, i])
+        )
+        scale = lax.rsqrt(jnp.mean(mix * mix, axis=-1, keepdims=True) + NORM_EPS)
+        gate = silu(og_v[:, lanes].astype(jnp.float32))
+        mixed[:, lanes] = (mix * scale * hgain_ref[...].astype(jnp.float32) * gate).astype(jnp.bfloat16)
+        return carry
+
+    lax.fori_loop(0, heads, mix_step, 0)
+    chunk = 512 if columns % 512 == 0 else width
+
+    def hidden_step(i, carry):
+        lanes = pl.ds(pl.multiple_of(i * chunk, chunk), chunk)
+        part = dot_nn(mixed[...], wo_v[:, lanes]).astype(jnp.bfloat16).astype(jnp.float32)
+        hidden = (res_v[:, lanes].astype(jnp.float32) + part).astype(jnp.bfloat16)
+        res_v[:, lanes] = hidden
+        hidden = hidden.astype(jnp.float32)
+        return carry + jnp.sum(hidden * hidden, axis=-1, keepdims=True)
+
+    squares = lax.fori_loop(0, columns // chunk, hidden_step, jnp.zeros((rows, 1), jnp.float32))
+    scale = lax.rsqrt(squares / columns + NORM_EPS)
+    tok[z] = (res_v[...].astype(jnp.float32) * scale * mgain_ref[...].astype(jnp.float32)).astype(jnp.bfloat16)
+
+    up_dev, dn_dev = me + side, me - side
+
+    def up(zz):
+        return copy(tok.at[zz], tok.at[zz], up_out.at[zz], up_in.at[zz], up_dev)
+
+    def dn(zz):
+        return copy(tok.at[zz], tok.at[zz], dn_out.at[zz], dn_in.at[zz], dn_dev)
+
+    @pl.when(z < nz - 1)
+    def _():
+        up(z).start()
+
+    @pl.when(z > 0)
+    def _():
+        dn(z).start()
+
+    def relay(k):
+        @pl.when(z - k >= 0)
+        def _():
+            up(z - k).wait_recv()
+
+            @pl.when(z < nz - 1)
+            def _():
+                up(z - k).start()
+
+        @pl.when(z + k < nz)
+        def _():
+            dn(z + k).wait_recv()
+
+            @pl.when(z > 0)
+            def _():
+                dn(z + k).start()
+
+    for k in range(3, nz):
+        spread(k)
+    for k in range(2, nz - 1):
+        onward(k)
+    relay(1)
+    for k in range(1, nz - 1):
+        last(k)
+    onward(nz - 1)
+    for k in range(2, nz):
+        relay(k)
+    last(nz - 1)
+    for k in range(nz):
+        for j in range(PLANE):
+            partner(k, j).wait_recv()
+
+    def give(k):
+        return copy(parts.at[k], terms.at[k], r_out.at[k], r_in.at[k], along[k])
+
+    def mixer(zz, slot):
+        block = tok[zz]
+        gate_act = dot_nn(block, w_v[0])
+        up_act = dot_nn(block, w_v[1])
+        inner = (silu(gate_act) * up_act).astype(jnp.bfloat16)
+        parts[slot] = dot_nt(inner, w_v[2]).astype(jnp.bfloat16)
+
+    def mixer_step(i, carry):
+        k = lax.rem(i + 1, nz)
+        zz = z
+        for j in range(1, nz):
+            zz = jnp.where(k == j, zs[j], zz)
+        mixer(zz, k)
+
+        for j in range(1, nz):
+            @pl.when(k == j)
+            def _(j=j):
+                give(j).start()
+
+        return carry
+
+    lax.fori_loop(0, nz, mixer_step, 0)
+    added = res_v[...].astype(jnp.float32) + parts[0].astype(jnp.float32)
+    for k in range(1, nz):
+        give(k).wait_recv()
+        added = added + terms[k].astype(jnp.float32)
+    out_ref[...] = added.astype(jnp.bfloat16)
+
+    for k in range(1, nz):
+        for one in first(k):
+            one.wait_send()
+        give(k).wait_send()
+
+        @pl.when(give_after(k))
+        def _(k=k):
+            total_copy(k).wait_send()
+    for k in range(nz):
+        plane(k, (x_out, x_in), x_dev).wait_send()
+        plane(k, (y_out, y_in), y_dev).wait_send()
+        corner(k).wait_send()
+        for j in range(PLANE):
+            partner(k, j).wait_send()
+
+        @pl.when(jnp.logical_and(z < nz - 1, k <= z))
+        def _(k=k):
+            up(k).wait_send()
+
+        @pl.when(jnp.logical_and(z > 0, k >= z))
+        def _(k=k):
+            dn(k).wait_send()
+    for w in range(side):
+        @pl.when(w != seat)
+        def _(w=w):
+            state_copy(w).wait_send()
+            enter_copy(w).wait_send()
+
+
+def layer(queries, forget_logits, values, gate_logits, slack, spike, head_gain, output_weight, residual, mixer_gain, gate, up, down):
+    n = lax.axis_size("sp")
+    nz = n // (PLANE * CORES)
+    rows, columns = queries.shape
+    heads, width = spike.shape[1], head_gain.shape[0]
+    depth, units = gate.shape[0], gate.shape[1] // nz
+    side = PLANE * CORES
+    per = 2 * heads // side
+    bf16, f32 = jnp.bfloat16, jnp.float32
+    anywhere = pl.BlockSpec(memory_space=pl.ANY)
+    near = pl.BlockSpec(memory_space=pltpu.VMEM)
+    dma = pltpu.SemaphoreType.DMA
+    return pl.pallas_call(
+        functools.partial(layer_kernel, nz),
+        in_specs=[anywhere] * 5 + [near] * 4 + [anywhere] * 4,
+        out_specs=near,
+        out_shape=jax.ShapeDtypeStruct((rows, columns), bf16),
+        scratch_shapes=[
+            pltpu.VMEM((rows, columns), bf16),
+            pltpu.VMEM((2, rows, columns), bf16),
+            pltpu.VMEM((rows, columns), bf16),
+            pltpu.VMEM((rows, columns), bf16),
+            pltpu.VMEM((rows, columns), bf16),
+            pltpu.VMEM(output_weight.shape, bf16),
+            pltpu.VMEM((3, n * depth, units), bf16),
+            pltpu.VMEM((2, rows, columns), bf16),
+            pltpu.VMEM((2, rows, columns), bf16),
+            pltpu.VMEM((rows, columns), f32),
+            pltpu.VMEM((side, per, width + PAD_ROWS, width), bf16),
+            pltpu.VMEM((side, per, width + PAD_ROWS, width), bf16),
+            pltpu.VMEM((per, width + PAD_ROWS, width), bf16),
+            pltpu.VMEM((nz, per, width + PAD_ROWS, width), bf16),
+            pltpu.VMEM((per, width, width), f32),
+            pltpu.VMEM((side, per, width, width), bf16),
+            pltpu.VMEM((side, per, width, width), bf16),
+            pltpu.VMEM((rows, columns), bf16),
+            pltpu.VMEM((nz, rows, columns), bf16),
+            pltpu.VMEM((nz, rows, columns), bf16),
+            pltpu.VMEM((nz, rows, columns), bf16),
+            dma((6,)),
+            dma((3,)),
+            dma((3, nz)),
+            dma((3, nz)),
+            dma((nz,)), dma((nz,)), dma((nz,)), dma((nz,)), dma((nz,)), dma((nz,)),
+            dma((nz, PLANE)), dma((nz, PLANE)),
+            dma((side,)), dma((side,)),
+            dma((nz,)), dma((nz,)),
+            dma((side,)), dma((side,)),
+            dma((nz,)), dma((nz,)), dma((nz,)), dma((nz,)),
+            dma((nz,)), dma((nz,)),
+        ],
+        compiler_params=pltpu.CompilerParams(
+            collective_id=7, has_side_effects=True, vmem_limit_bytes=60 * 1024 * 1024
+        ),
+        name="layer",
+    )(
+        queries, forget_logits, values, gate_logits, residual, slack.reshape(1, columns), spike,
+        head_gain.reshape(1, width), mixer_gain.reshape(1, columns), output_weight, gate, up, down.T,
+    )
+
+
 def local(
     queries,
     forget_logits,
@@ -369,6 +850,23 @@
     mixer_down_weight,
 ):
     n, tp = lax.axis_size("sp"), lax.axis_size("tp")
+    nz, tail = n // (PLANE * CORES), n % (PLANE * CORES)
+    if tp == 1 and tail == 0 and nz in (2, 4) and mixer_gate_weight.shape[1] % (128 * nz) == 0:
+        return layer(
+            queries,
+            forget_logits,
+            value_matrix,
+            output_gate_logits,
+            forget_slack,
+            spike_log_forget,
+            head_norm_gain,
+            output_weight,
+            residual,
+            mixer_norm_gain,
+            mixer_gate_weight,
+            mixer_up_weight,
+            mixer_down_weight,
+        )
     g = GROUP
     row_count = queries.shape[0]
     depth, units = mixer_gate_weight.shape

time: 359 us -> 174 us (0.48); the launches traced: 353 us -> 173 us
  Pallas kernels: 264 us -> 168 us
  waiting for transfers between devices: 44.2 us -> 0 us
  matrix products: 17.9 us -> 0 us
  between operations: 13.3 us -> 0.01 us
  other arithmetic: 7.38 us -> 0 us
    pallas_call x6 -> x1, Pallas kernels: 264 us -> 168 us  [layer(): pl.pallas_call(functools.partial(layer_kernel, nz), in_specs=[anywhere] *...]
    all_gather x3 -> x0, waiting for transfers between devices: 42.8 us -> none  [local(): lax.all_gather(p.reshape(g * depth, units // g), 'sp', axis=0, tiled=True...]
    dot_general x2 -> x0, matrix products: 17.9 us -> none  [the longest x1 11.9 us: dot_nt(): lax.dot_general(a, b, (((1,), (1,)), ((), ())), preferred_element_type=jn...]
    reduce_sum x2 -> x0, other arithmetic: 4.34 us -> none  [the longest x1 3.04 us: local(): added = jnp.sum(terms.astype(jnp.float32), axis=0)]
  transfers between devices with their start and end apart: 3 -> 0, of which waited for: 1 -> 0; matrix products, arithmetic and copies ran while one was open for 3% -> 0% of each run, Pallas kernels for 51% -> 0%
where the time goes in v1:
time: 174 us; the launch traced here: 173 us
  Pallas kernels  168 us (97%)
  local copies, waits for them, and re-layouts  4.59 us (3%)
    pallas_call x1, Pallas kernels, layer(): pl.pallas_call(functools.partial(layer_kernel, nz), in_specs=[anywhere] *...  168 us

profile of v1, /device:TPU:8, one launch (start us, length us, event | category | flops | bytes accessed | tf_op | source)
XLA Modules:
  0.0 172.7 jit_solution(15024830537091912202)
XLA Ops:
  0.0 1.3 reshape.11.mgain_ref
  1.3 1.4 copy.14.spike_ref
  2.7 168.1 %layer.1 = bf16[128,2048]{1,0:T(8,128)(2,1)} custom-call(bf16[128,2048]{1,0:T(8,128)(2,1)} %q_hbm.1, bf16[2,128,2048]{2,1,0:T(8,128)(2,1)} %f_hbm.1, bf16[128,2048]{1,0:T(8,128)(2,1)} %v_hbm.1, bf16[128,2048]{1,0:T(8,128)(2,1)} %og_hbm.1, bf16[128,2048]{1,0:T(8,128)(2,1)} %res_hbm.1, f32[1,2048]{1,0:T(1,128)} %bitcast.4, f32[128,16]{1,0:T(8,128)} %copy.14.spike_ref, ...), custom_call_target="tpu_custom_call" | custom-call | tf_op jit(solution)/shard_map/layer/pallas_call | solution.py:788
  170.8 1.9 %copy.16 = bf16[128,2048]{1,0:T(8,128)(2,1)} copy(bf16[128,2048]{1,0:T(8,128)(2,1)} %layer.1) | data formatting | bytes 1048576

commit v2 on v0

--- a/solution.py
+++ b/solution.py
@@ -353,6 +353,632 @@
     )(local, reach, entered, gain.reshape(1, width), gate_logits, weight)
 
 
+CORES = 2
+PLANE = 4
+
+
+def flip(i, k):
+    out, bit = i, 1
+    while bit <= k:
+        if k & bit:
+            out = out + bit - 2 * bit * (lax.rem(i // bit, 2))
+        bit *= 2
+    return out
+
+
+def layer_kernel(
+    nz,
+    q_hbm, f_hbm, v_hbm, og_hbm, res_hbm, slack_ref, spike_ref, hgain_ref, mgain_ref, wo_hbm, gate_hbm, up_hbm, down_hbm,
+    out_ref,
+    q_v, f_v, v_v, og_v, res_v, wo_v, w_v,
+    reach, scaled, locals_, states, mate, chip, held, total, totals_in, entry, made, enter, beside, mixed, tok, inner,
+    parts, terms,
+    in_sem, w0_sem, w1_out, w1_in, x_out, x_in, y_out, y_in, d_out, d_in, p_out, p_in,
+    s0_out, s0_in, s1_out, s1_in, s2_out, s2_in, s3_out, s3_in, s4_out, s4_in,
+    up_out, up_in, dn_out, dn_in, r_out, r_in,
+):
+    rows, columns = q_v.shape
+    width = hgain_ref.shape[1]
+    heads = columns // width
+    depth = gate_hbm.shape[0]
+    units = w_v.shape[2]
+    side = PLANE * CORES
+    per = heads // PLANE
+    me = lax.axis_index("sp")
+    z, seat = me // side, lax.rem(me, side)
+    q, c = seat // CORES, lax.rem(seat, CORES)
+
+    def at(zz, qq, cc):
+        return zz * side + qq * CORES + cc
+
+    def copy(src, dst, out_sem, got_sem, there):
+        return pltpu.make_async_remote_copy(
+            src_ref=src, dst_ref=dst, send_sem=out_sem, recv_sem=got_sem,
+            device_id={"sp": there}, device_id_type=MESH,
+        )
+
+    def when(condition, act):
+        pl.when(condition)(act)
+
+    zs = [z] + [flip(z, k) for k in range(1, nz)]
+    qs = [q] + [flip(q, k) for k in range(1, PLANE)]
+    along = [at(zz, q, c) for zz in zs]
+    x_dev, y_dev, p_dev = at(z, qs[1], c), at(z, qs[2], c), at(z, q, 1 - c)
+    up_dev, dn_dev = me + side, me - side
+
+    loads = [
+        pltpu.make_async_copy(src, dst, in_sem.at[i])
+        for i, (src, dst) in enumerate(
+            ((f_hbm, f_v), (q_hbm, q_v), (v_hbm, v_v), (og_hbm, og_v), (res_hbm, res_v), (wo_hbm, wo_v))
+        )
+    ]
+    weights = (gate_hbm, up_hbm, down_hbm)
+
+    def cut(a, zz):
+        return weights[a].at[:, pl.ds(pl.multiple_of(zz * units, 128), units)]
+
+    def strip(a, device):
+        return w_v.at[a, pl.ds(pl.multiple_of(device * depth, depth), depth), :]
+
+    own = [pltpu.make_async_copy(cut(a, z), strip(a, me), w0_sem.at[a]) for a in range(3)]
+    for load in loads[:3]:
+        load.start()
+    for load in own:
+        load.start()
+
+    barrier = pltpu.get_barrier_semaphore()
+    for k in range(1, nz):
+        pl.semaphore_signal(barrier, inc=1, device_id={"sp": along[k]}, device_id_type=MESH)
+    for k in range(1, side):
+        pl.semaphore_signal(
+            barrier, inc=1, device_id={"sp": z * side + lax.rem(seat + k, side)}, device_id_type=MESH
+        )
+    pl.semaphore_wait(barrier, nz - 1 + side - 1)
+
+    members = ((0, 1), (2,))
+
+    outer = jnp.logical_or(z == 0, z == nz - 1)
+    order = [z] + [jnp.where(outer, zs[i], zs[j]) for i, j in ((1, 2), (3, 1), (2, 3))]
+
+    def source(part, k):
+        return order[k] if part == 0 else k
+
+    def first(part, k):
+        return [
+            copy(cut(a, zs[k]), strip(a, me), w1_out.at[0], w1_in.at[a, z], along[k]) for a in members[part]
+        ]
+
+    def first_start(*which):
+        for part, k in which:
+            for one in first(part, k):
+                one.start()
+
+    def first_wait(part, k):
+        origin = source(part, k)
+
+        @pl.when(origin != z)
+        def _():
+            for a in members[part]:
+                copy(cut(a, z), strip(a, me), w1_out.at[0], w1_in.at[a, origin], along[1]).wait_recv()
+
+    def piece(part, k, j):
+        row = pl.multiple_of(at(source(part, k), qs[j], c) * depth, depth)
+        lo, count = members[part][0], len(members[part])
+        return w_v.at[pl.ds(lo, count), pl.ds(row, depth), :]
+
+    def across_x(part, k):
+        src = piece(part, k, 0)
+        return copy(src, src, x_out.at[0], x_in.at[part, k], x_dev)
+
+    def across_y(part, k):
+        src = piece(part, k, 0)
+        return copy(src, src, y_out.at[0], y_in.at[part, k], y_dev)
+
+    def corner(part, k):
+        near, there = (1, y_dev) if k < nz // 2 else (2, x_dev)
+        src = piece(part, k, near)
+        return copy(src, src, d_out.at[0], d_in.at[part, k], there)
+
+    def partner(part, k, j):
+        src = piece(part, k, j)
+        return copy(src, src, p_out.at[0], p_in.at[part, k, j], p_dev)
+
+    def spread(part, k):
+        if part == 0 and k == 0:
+            for a in members[0]:
+                own[a].wait()
+        else:
+            first_wait(part, k)
+        across_x(part, k).start()
+        across_y(part, k).start()
+        partner(part, k, 0).start()
+
+    def onward(part, k):
+        across_x(part, k).wait_recv()
+        if k < nz // 2:
+            corner(part, k).start()
+        partner(part, k, 1).start()
+        across_y(part, k).wait_recv()
+        if k >= nz // 2:
+            corner(part, k).start()
+        partner(part, k, 2).start()
+
+    def last(part, k):
+        corner(part, k).wait_recv()
+        partner(part, k, 3).start()
+
+    def settle(part, k):
+        for j in range(PLANE):
+            partner(part, k, j).wait_recv()
+
+    when(outer, lambda: first_start((0, 2), (0, 3)))
+    when(jnp.logical_not(outer), lambda: first_start((0, 1)))
+    spread(0, 0)
+    for load in loads[3:]:
+        load.start()
+
+    down = lax.broadcasted_iota(jnp.int32, (rows, rows), 0)
+    sideways = lax.broadcasted_iota(jnp.int32, (rows, rows), 1)
+    masks = (down >= sideways, down <= sideways)
+    for load in loads[:3]:
+        load.wait()
+    spikes = jnp.transpose(spike_ref[...])
+    lane = lax.broadcasted_iota(jnp.int32, spikes.shape, 1)
+    place = lax.broadcasted_iota(jnp.int32, (PAD_ROWS, width), 0)
+
+    def pad(decay):
+        high, low = split_bf16(decay)
+        return jnp.where(
+            place == 0, high.astype(jnp.float32), jnp.where(place == 1, low.astype(jnp.float32), 0.0)
+        ).astype(jnp.bfloat16)
+
+    def unpack(block):
+        block = block.astype(jnp.float32)
+        return block[:, width : width + 1] + block[:, width + 1 : width + 2], block[:, :width]
+
+    def by_head(head):
+        return pl.ds(pl.multiple_of(head * width, width), width)
+
+    def make_states(group):
+        def step(i, carry):
+            head = group * per + i
+            lanes = by_head(head)
+            query = silu(q_v[:, lanes].astype(jnp.float32)) * (width ** -0.5)
+            value = v_v[:, lanes]
+            spike = jnp.sum(jnp.where(lane == head, spikes, 0.0), axis=1, keepdims=True)
+            slack = slack_ref[:, lanes]
+            for way in (0, 1):
+                tri = jnp.where(masks[way], 1.0, 0.0).astype(jnp.bfloat16)
+                key = slack * jax.nn.sigmoid(-f_v[way, :, lanes].astype(jnp.float32))
+                decay = jnp.log1p(-key) + spike
+                high, low = split_bf16(decay)
+                running = dot_nn(tri, high) + dot_nn(tri, low)
+                final = running[rows - 1 : rows] if way == 0 else running[0:1]
+                reach[way, :, lanes] = (query * jnp.exp(running)).astype(jnp.bfloat16)
+                scaled[way, :, lanes] = (key * jnp.exp(-running)).astype(jnp.bfloat16)
+                key_end = (key * jnp.exp(final - running)).astype(jnp.bfloat16)
+                states[way, group, i, 0:width] = dot_tn(value, key_end).astype(jnp.bfloat16)
+                states[way, group, i, width : width + PAD_ROWS] = pad(jnp.exp(final))
+            return carry
+
+        lax.fori_loop(0, per, step, 0)
+
+    def mate_copy(group):
+        return copy(states.at[1 - c, group], mate.at[group], s0_out.at[group], s0_in.at[group], p_dev)
+
+    def chip_copy(group):
+        return copy(chip.at[group], held.at[q], s1_out.at[group], s1_in.at[q], at(z, group, c))
+
+    def chip_arrival(group):
+        return copy(chip.at[group], held.at[group], s1_out.at[group], s1_in.at[group], at(z, group, c))
+
+    def join(group):
+        mate_copy(group).wait_recv()
+        factor, state = unpack(states[c, group])
+        mate_factor, mate_state = unpack(mate[group])
+        chip[group, :, 0:width] = (mate_factor * state + mate_state).astype(jnp.bfloat16)
+        both = factor * mate_factor
+        for i in range(per):
+            chip[group, i, width : width + PAD_ROWS] = pad(both[i])
+        when(q != group, lambda: chip_copy(group).start())
+
+        @pl.when(q == group)
+        def _():
+            held[group] = chip[group]
+
+    def local_step(head, carry):
+        lanes = by_head(head)
+        scores = None
+        for way in (0, 1):
+            part = jnp.where(masks[way], dot_nt(reach[way, :, lanes], scaled[way, :, lanes]), 0.0)
+            scores = part if scores is None else scores + part
+        locals_[:, lanes] = dot_nn(scores.astype(jnp.bfloat16), v_v[:, lanes])
+        return carry
+
+    for group in range(PLANE):
+        make_states(group)
+        mate_copy(group).start()
+        if group > 0:
+            join(group - 1)
+    lax.fori_loop(0, heads // 2, local_step, 0)
+    join(PLANE - 1)
+    lax.fori_loop(heads // 2, heads, local_step, 0)
+    onward(0, 0)
+
+    for w in range(PLANE):
+        when(w != q, lambda w=w: chip_arrival(w).wait_recv())
+
+    def turn(i, count):
+        return i + c * (count - 1 - 2 * i)
+
+    entry[...] = jnp.zeros_like(entry)
+    decay = jnp.ones((per, 1, width), jnp.float32)
+    for i in range(PLANE):
+        factor, state = unpack(held[turn(i, PLANE)])
+        entry[...] = factor * entry[...] + state
+        decay = factor * decay
+    total[:, 0:width] = entry[...].astype(jnp.bfloat16)
+    for i in range(per):
+        total[i, width : width + PAD_ROWS] = pad(decay[i])
+
+    def give_after(k):
+        return (zs[k] > z) == (c == 0)
+
+    def total_copy(k):
+        return copy(total, totals_in.at[z], s2_out.at[k], s2_in.at[k], along[k])
+
+    for k in range(1, nz):
+        when(give_after(k), lambda k=k: total_copy(k).start())
+    when(outer, lambda: first_start((0, 1)))
+    own[2].wait()
+    when(jnp.logical_not(outer), lambda: first_start((0, 3), (0, 2), (1, 1), (1, 3), (1, 2)))
+    spread(0, 1)
+    entry[...] = jnp.zeros_like(entry)
+    for k in range(1, nz):
+        when(jnp.logical_not(give_after(k)), lambda k=k: total_copy(k).wait_recv())
+    for i in range(nz):
+        origin = turn(i, nz)
+
+        @pl.when(jnp.logical_and(origin != z, (origin < z) == (c == 0)))
+        def _(origin=origin):
+            factor, state = unpack(totals_in[origin])
+            entry[...] = factor * entry[...] + state
+
+    def enter_copy(w):
+        return copy(made.at[w], enter.at[c, q], s3_out.at[w], s3_in.at[q], at(z, w, c))
+
+    def enter_arrival(w):
+        return copy(made.at[w], enter.at[c, w], s3_out.at[w], s3_in.at[w], at(z, w, c))
+
+    def beside_copy(group):
+        return copy(beside.at[group], enter.at[c, group], s4_out.at[group], s4_in.at[group], p_dev)
+
+    def beside_arrival(group):
+        return copy(beside.at[group], enter.at[1 - c, group], s4_out.at[group], s4_in.at[group], p_dev)
+
+    for i in range(PLANE):
+        origin = turn(i, PLANE)
+        made[origin] = entry[...].astype(jnp.bfloat16)
+        when(origin != q, lambda origin=origin: enter_copy(origin).start())
+        factor, state = unpack(held[origin])
+        entry[...] = factor * entry[...] + state
+    enter[c, q] = made[q]
+    onward(0, 1)
+    when(outer, lambda: first_start((1, 2), (1, 3), (1, 1)))
+    last(0, 0)
+    spread(0, 2)
+    for w in range(PLANE):
+        when(w != q, lambda w=w: enter_arrival(w).wait_recv())
+        factor, state = unpack(states[c, w])
+        beside[w] = (factor * enter[c, w].astype(jnp.float32) + state).astype(jnp.bfloat16)
+        beside_copy(w).start()
+    for load in loads[3:]:
+        load.wait()
+    for w in range(PLANE):
+        beside_arrival(w).wait_recv()
+
+    def mix_step(head, carry):
+        lanes = by_head(head)
+        group, i = head // per, lax.rem(head, per)
+        mix = (
+            locals_[:, lanes]
+            + dot_nt(reach[0, :, lanes], enter[0, group, i])
+            + dot_nt(reach[1, :, lanes], enter[1, group, i])
+        )
+        scale = lax.rsqrt(jnp.mean(mix * mix, axis=-1, keepdims=True) + NORM_EPS)
+        gate = silu(og_v[:, lanes].astype(jnp.float32))
+        mixed[:, lanes] = (mix * scale * hgain_ref[...].astype(jnp.float32) * gate).astype(jnp.bfloat16)
+        return carry
+
+    lax.fori_loop(0, heads, mix_step, 0)
+    chunk = columns // nz
+
+    def hidden_step(i, carry):
+        lanes = pl.ds(pl.multiple_of(i * chunk, chunk), chunk)
+        part = dot_nn(mixed[...], wo_v[:, lanes]).astype(jnp.bfloat16).astype(jnp.float32)
+        hidden = (res_v[:, lanes].astype(jnp.float32) + part).astype(jnp.bfloat16)
+        res_v[:, lanes] = hidden
+        hidden = hidden.astype(jnp.float32)
+        return carry + jnp.sum(hidden * hidden, axis=-1, keepdims=True)
+
+    squares = lax.fori_loop(0, columns // chunk, hidden_step, jnp.zeros((rows, 1), jnp.float32))
+    scale = lax.rsqrt(squares / columns + NORM_EPS)
+    for i in range(columns // width):
+        lanes = pl.ds(i * width, width)
+        gain = mgain_ref[i : i + 1].astype(jnp.float32)
+        tok[z, :, lanes] = (res_v[:, lanes].astype(jnp.float32) * scale * gain).astype(jnp.bfloat16)
+
+    def half(zz, h):
+        return tok.at[zz, :, pl.ds(h * (columns // 2), columns // 2)]
+
+    def up(zz, h):
+        return copy(half(zz, h), half(zz, h), up_out.at[zz, h], up_in.at[zz, h], up_dev)
+
+    def dn(zz, h):
+        return copy(half(zz, h), half(zz, h), dn_out.at[zz, h], dn_in.at[zz, h], dn_dev)
+
+    for h in (0, 1):
+        when(z < nz - 1, lambda h=h: up(z, h).start())
+        when(z > 0, lambda h=h: dn(z, h).start())
+
+    def relay(k, h):
+        @pl.when(z - k >= 0)
+        def _():
+            up(z - k, h).wait_recv()
+            when(z < nz - 1, lambda: up(z - k, h).start())
+
+        @pl.when(z + k < nz)
+        def _():
+            dn(z + k, h).wait_recv()
+            when(z > 0, lambda: dn(z + k, h).start())
+
+    def expand(zz):
+        block = tok[zz]
+        gate_act = dot_nn(block, w_v[0])
+        up_act = dot_nn(block, w_v[1])
+        inner[zz] = (silu(gate_act) * up_act).astype(jnp.bfloat16)
+
+    def ordered(i):
+        reach_dn, reach_up = z, nz - 1 - z
+        near = jnp.minimum(reach_dn, reach_up)
+        pair = (i + 1) // 2
+        odd = lax.rem(i, 2)
+        both = z + jnp.where(odd == 1, -pair, pair)
+        single = jnp.where(reach_dn < reach_up, i, nz - 1 - i)
+        return jnp.where(pair <= near, both, single)
+
+    def lanes_of(s):
+        return pl.ds(s * chunk, chunk)
+
+    def lower(zz, s):
+        out = dot_nt(inner[zz], w_v[2, s * chunk : (s + 1) * chunk])
+        parts[zz, :, lanes_of(s)] = out.astype(jnp.bfloat16)
+
+    def sum_up(zz, s):
+        return copy(
+            parts.at[zz, :, lanes_of(s)], terms.at[0, zz, :, lanes_of(s)], r_out.at[0], r_in.at[0, zz, s], up_dev
+        )
+
+    def sum_dn(zz, s):
+        return copy(
+            parts.at[zz, :, lanes_of(s)], terms.at[1, zz, :, lanes_of(s)], r_out.at[0], r_in.at[1, zz, s], dn_dev
+        )
+
+    def take(way, zz, s):
+        (sum_up, sum_dn)[way](zz, s).wait_recv()
+        parts[zz, :, lanes_of(s)] = (
+            parts[zz, :, lanes_of(s)].astype(jnp.float32) + terms[way, zz, :, lanes_of(s)].astype(jnp.float32)
+        ).astype(jnp.bfloat16)
+
+    def ends(s, *far):
+        for d in far:
+            when(z == 0, lambda d=d: sum_up(d, s).start())
+            when(z == nz - 1, lambda d=d: sum_dn(nz - 1 - d, s).start())
+
+    def pass_up(at_z, zz, s):
+        @pl.when(z == at_z)
+        def _():
+            take(0, zz, s)
+            sum_up(zz, s).start()
+
+    def pass_dn(at_z, zz, s):
+        @pl.when(z == at_z)
+        def _():
+            take(1, zz, s)
+            sum_dn(zz, s).start()
+
+    def near_pass(s):
+        pass_up(1, 2, s)
+        pass_dn(2, 1, s)
+
+    def far_pass(s):
+        pass_up(1, 3, s)
+        pass_dn(2, 0, s)
+
+    def end_pass(s):
+        pass_up(2, 3, s)
+        pass_dn(1, 0, s)
+
+    def work(lo, hi, act):
+        def step(i, carry):
+            act(ordered(i))
+            return carry
+
+        lax.fori_loop(lo, hi, step, 0)
+
+    spread(0, 3)
+    onward(0, 2)
+    spread(1, 0)
+    last(0, 1)
+    relay(1, 0)
+    onward(0, 3)
+    spread(1, 1)
+    last(0, 2)
+    settle(0, 0)
+    settle(0, 1)
+    relay(1, 1)
+    onward(1, 0)
+    spread(1, 2)
+    last(0, 3)
+    relay(2, 0)
+    settle(0, 2)
+    settle(0, 3)
+    work(0, 1, expand)
+    onward(1, 1)
+    spread(1, 3)
+    work(1, 2, expand)
+    relay(2, 1)
+    last(1, 0)
+    work(2, 3, expand)
+    settle(1, 0)
+    work(0, 3, lambda zz: lower(zz, 0))
+    ends(0, 1, 2)
+    onward(1, 2)
+    last(1, 1)
+    settle(1, 1)
+    work(0, 3, lambda zz: lower(zz, 1))
+    ends(1, 1, 2)
+    near_pass(0)
+    onward(1, 3)
+    last(1, 2)
+    settle(1, 2)
+    work(0, 3, lambda zz: lower(zz, 2))
+    ends(2, 1, 2)
+    near_pass(1)
+    relay(3, 0)
+    relay(3, 1)
+    work(3, 4, expand)
+    for s in range(3):
+        work(3, 4, lambda zz, s=s: lower(zz, s))
+        ends(s, 3)
+    last(1, 3)
+    settle(1, 3)
+    near_pass(2)
+    far_pass(0)
+    work(0, 4, lambda zz: lower(zz, 3))
+    ends(3, 3, 2, 1)
+    far_pass(1)
+    end_pass(0)
+    far_pass(2)
+    end_pass(1)
+    far_pass(3)
+    near_pass(3)
+    end_pass(2)
+    end_pass(3)
+
+    def finish(s):
+        when(z > 0, lambda: sum_up(z, s).wait_recv())
+        when(z < nz - 1, lambda: sum_dn(z, s).wait_recv())
+        lanes = lanes_of(s)
+        added = res_v[:, lanes].astype(jnp.float32) + parts[z, :, lanes].astype(jnp.float32)
+        added = added + jnp.where(z > 0, terms[0, z, :, lanes].astype(jnp.float32), 0.0)
+        added = added + jnp.where(z < nz - 1, terms[1, z, :, lanes].astype(jnp.float32), 0.0)
+        out_ref[:, lanes] = added.astype(jnp.bfloat16)
+
+    for s in range(nz):
+        finish(s)
+
+    def sent(src, sem, got_sem, there):
+        copy(src, src, sem, got_sem, there).wait_send()
+
+    sent(w_v.at[:, 0 : (nz - 1) * depth], w1_out.at[0], w1_in.at[0, 0], x_dev)
+    sent(w_v.at[:, 0 : nz * depth], x_out.at[0], x_in.at[0, 0], x_dev)
+    sent(w_v.at[:, 0 : nz * depth], y_out.at[0], y_in.at[0, 0], y_dev)
+    sent(w_v.at[:, 0 : nz * depth], d_out.at[0], d_in.at[0, 0], x_dev)
+    sent(w_v.at[:, 0 : PLANE * nz * depth], p_out.at[0], p_in.at[0, 0, 0], p_dev)
+    sent(parts.at[0 : nz - 1], r_out.at[0], r_in.at[0, 0, 0], x_dev)
+    for k in range(1, nz):
+        when(give_after(k), lambda k=k: total_copy(k).wait_send())
+    for k in range(nz):
+        for h in (0, 1):
+            when(jnp.logical_and(z < nz - 1, k <= z), lambda k=k, h=h: up(k, h).wait_send())
+            when(jnp.logical_and(z > 0, k >= z), lambda k=k, h=h: dn(k, h).wait_send())
+    for w in range(PLANE):
+        mate_copy(w).wait_send()
+        beside_copy(w).wait_send()
+
+        @pl.when(w != q)
+        def _(w=w):
+            chip_copy(w).wait_send()
+            enter_copy(w).wait_send()
+
+
+def layer(queries, forget_logits, values, gate_logits, slack, spike, head_gain, output_weight, residual, mixer_gain, gate, up, down):
+    n = lax.axis_size("sp")
+    nz = n // (PLANE * CORES)
+    rows, columns = queries.shape
+    heads, width = spike.shape[1], head_gain.shape[0]
+    depth, units = gate.shape[0], gate.shape[1] // nz
+    per = heads // PLANE
+    bf16, f32 = jnp.bfloat16, jnp.float32
+    anywhere = pl.BlockSpec(memory_space=pl.ANY)
+    near = pl.BlockSpec(memory_space=pltpu.VMEM)
+    dma = pltpu.SemaphoreType.DMA
+    padded = width + PAD_ROWS
+
+    def pairs(*shape):
+        return [dma(shape), dma(shape)]
+
+    def one_out(*shape):
+        return [dma((1,)), dma(shape)]
+
+    return pl.pallas_call(
+        functools.partial(layer_kernel, nz),
+        in_specs=[anywhere] * 5 + [near] * 4 + [anywhere] * 4,
+        out_specs=near,
+        out_shape=jax.ShapeDtypeStruct((rows, columns), bf16),
+        scratch_shapes=[
+            pltpu.VMEM((rows, columns), bf16),
+            pltpu.VMEM((2, rows, columns), bf16),
+            pltpu.VMEM((rows, columns), bf16),
+            pltpu.VMEM((rows, columns), bf16),
+            pltpu.VMEM((rows, columns), bf16),
+            pltpu.VMEM(output_weight.shape, bf16),
+            pltpu.VMEM((3, n * depth, units), bf16),
+            pltpu.VMEM((2, rows, columns), bf16),
+            pltpu.VMEM((2, rows, columns), bf16),
+            pltpu.VMEM((rows, columns), f32),
+            pltpu.VMEM((2, PLANE, per, padded, width), bf16),
+            pltpu.VMEM((PLANE, per, padded, width), bf16),
+            pltpu.VMEM((PLANE, per, padded, width), bf16),
+            pltpu.VMEM((PLANE, per, padded, width), bf16),
+            pltpu.VMEM((per, padded, width), bf16),
+            pltpu.VMEM((nz, per, padded, width), bf16),
+            pltpu.VMEM((per, width, width), f32),
+            pltpu.VMEM((PLANE, per, width, width), bf16),
+            pltpu.VMEM((2, PLANE, per, width, width), bf16),
+            pltpu.VMEM((PLANE, per, width, width), bf16),
+            pltpu.VMEM((rows, columns), bf16),
+            pltpu.VMEM((nz, rows, columns), bf16),
+            pltpu.VMEM((nz, rows, units), bf16),
+            pltpu.VMEM((nz, rows, columns), bf16),
+            pltpu.VMEM((2, nz, rows, columns), bf16),
+            dma((6,)),
+            dma((3,)),
+            *one_out(3, nz),
+            *one_out(2, nz),
+            *one_out(2, nz),
+            *one_out(2, nz),
+            *one_out(2, nz, PLANE),
+            *pairs(PLANE),
+            *pairs(PLANE),
+            *pairs(nz),
+            *pairs(PLANE),
+            *pairs(PLANE),
+            *pairs(nz, 2),
+            *pairs(nz, 2),
+            *one_out(2, nz, nz),
+        ],
+        compiler_params=pltpu.CompilerParams(
+            collective_id=7, has_side_effects=True, vmem_limit_bytes=60 * 1024 * 1024
+        ),
+        name="layer",
+    )(
+        queries, forget_logits, values, gate_logits, residual, slack.reshape(1, columns), spike.T,
+        head_gain.reshape(1, width), mixer_gain.reshape(columns // width, width), output_weight, gate, up, down.T,
+    )
+
+
 def local(
     queries,
     forget_logits,
@@ -369,6 +995,23 @@
     mixer_down_weight,
 ):
     n, tp = lax.axis_size("sp"), lax.axis_size("tp")
+    nz, tail = n // (PLANE * CORES), n % (PLANE * CORES)
+    if tp == 1 and tail == 0 and nz == PLANE and mixer_gate_weight.shape[1] % (128 * nz) == 0:
+        return layer(
+            queries,
+            forget_logits,
+            value_matrix,
+            output_gate_logits,
+            forget_slack,
+            spike_log_forget,
+            head_norm_gain,
+            output_weight,
+            residual,
+            mixer_norm_gain,
+            mixer_gate_weight,
+            mixer_up_weight,
+            mixer_down_weight,
+        )
     g = GROUP
     row_count = queries.shape[0]
     depth, units = mixer_gate_weight.shape

time: 359 us -> 143 us (0.40)
  the two profiles are of different devices: /device:TPU:8 before, /device:TPU:4 now
where the time goes in v2:
time: 143 us
  Pallas kernels  141 us (99%)
  local copies, waits for them, and re-layouts  1.88 us (1%)
    pallas_call x1, Pallas kernels, layer(): pl.pallas_call(functools.partial(layer_kernel, nz), in_specs=[anywhere] *...  141 us

profile of v2, /device:TPU:4, one launch (start us, length us, event | category | flops | bytes accessed | tf_op | source)
XLA Modules:
  0.0 142.5 jit_solution(17496647347813221127)
XLA Ops:
  0.0 140.6 %layer.1 = bf16[128,2048]{1,0:T(8,128)(2,1)} custom-call(bf16[128,2048]{1,0:T(8,128)(2,1)} %q_hbm.1, bf16[2,128,2048]{2,1,0:T(8,128)(2,1)} %f_hbm.1, bf16[128,2048]{1,0:T(8,128)(2,1)} %v_hbm.1, bf16[128,2048]{1,0:T(8,128)(2,1)} %og_hbm.1, bf16[128,2048]{1,0:T(8,128)(2,1)} %res_hbm.1, f32[1,2048]{1,0:T(1,128)} %bitcast.6, f32[16,128]{1,0:T(8,128)} %bitcast.7, ...), custom_call_target="tpu_custom_call" | custom-call | tf_op jit(solution)/shard_map/layer/pallas_call | solution.py:925
  140.6 1.9 %copy.15 = bf16[128,2048]{1,0:T(8,128)(2,1)} copy(bf16[128,2048]{1,0:T(8,128)(2,1)} %layer.1) | data formatting | bytes 1048576

commit v3 on v2

--- a/solution.py
+++ b/solution.py
@@ -371,7 +371,7 @@
     q_hbm, f_hbm, v_hbm, og_hbm, res_hbm, slack_ref, spike_ref, hgain_ref, mgain_ref, wo_hbm, gate_hbm, up_hbm, down_hbm,
     out_ref,
     q_v, f_v, v_v, og_v, res_v, wo_v, w_v,
-    reach, scaled, locals_, states, mate, chip, held, total, totals_in, entry, made, enter, beside, mixed, tok, inner,
+    reach, scaled, locals_, gates, states, mate, chip, held, total, totals_in, entry, made, enter, beside, mixed, tok, inner,
     parts, terms,
     in_sem, w0_sem, w1_out, w1_in, x_out, x_in, y_out, y_in, d_out, d_in, p_out, p_in,
     s0_out, s0_in, s1_out, s1_in, s2_out, s2_in, s3_out, s3_in, s4_out, s4_in,
@@ -438,7 +438,7 @@
     members = ((0, 1), (2,))
 
     outer = jnp.logical_or(z == 0, z == nz - 1)
-    order = [z] + [jnp.where(outer, zs[i], zs[j]) for i, j in ((1, 2), (3, 1), (2, 3))]
+    order = (zs[0], zs[1], zs[3], zs[2])
 
     def source(part, k):
         return order[k] if part == 0 else k
@@ -511,8 +511,7 @@
         for j in range(PLANE):
             partner(part, k, j).wait_recv()
 
-    when(outer, lambda: first_start((0, 2), (0, 3)))
-    when(jnp.logical_not(outer), lambda: first_start((0, 1)))
+    first_start((0, 1), (0, 3))
     spread(0, 0)
     for load in loads[3:]:
         load.start()
@@ -550,18 +549,20 @@
             for way in (0, 1):
                 tri = jnp.where(masks[way], 1.0, 0.0).astype(jnp.bfloat16)
                 key = slack * jax.nn.sigmoid(-f_v[way, :, lanes].astype(jnp.float32))
-                decay = jnp.log1p(-key) + spike
+                decay = jnp.log(1.0 - key) + spike
                 high, low = split_bf16(decay)
                 running = dot_nn(tri, high) + dot_nn(tri, low)
                 final = running[rows - 1 : rows] if way == 0 else running[0:1]
                 reach[way, :, lanes] = (query * jnp.exp(running)).astype(jnp.bfloat16)
-                scaled[way, :, lanes] = (key * jnp.exp(-running)).astype(jnp.bfloat16)
-                key_end = (key * jnp.exp(final - running)).astype(jnp.bfloat16)
+                key = key * jnp.exp(-running)
+                scaled[way, :, lanes] = key.astype(jnp.bfloat16)
+                final = jnp.exp(final)
+                key_end = (key * final).astype(jnp.bfloat16)
                 states[way, group, i, 0:width] = dot_tn(value, key_end).astype(jnp.bfloat16)
-                states[way, group, i, width : width + PAD_ROWS] = pad(jnp.exp(final))
+                states[way, group, i, width : width + PAD_ROWS] = pad(final)
             return carry
 
-        lax.fori_loop(0, per, step, 0)
+        lax.fori_loop(0, per, step, 0, unroll=True)
 
     def mate_copy(group):
         return copy(states.at[1 - c, group], mate.at[group], s0_out.at[group], s0_in.at[group], p_dev)
@@ -600,10 +601,11 @@
         mate_copy(group).start()
         if group > 0:
             join(group - 1)
-    lax.fori_loop(0, heads // 2, local_step, 0)
+    lax.fori_loop(0, heads // 2, local_step, 0, unroll=4)
     join(PLANE - 1)
-    lax.fori_loop(heads // 2, heads, local_step, 0)
     onward(0, 0)
+    spread(0, 1)
+    lax.fori_loop(heads // 2, heads, local_step, 0, unroll=4)
 
     for w in range(PLANE):
         when(w != q, lambda w=w: chip_arrival(w).wait_recv())
@@ -627,12 +629,18 @@
     def total_copy(k):
         return copy(total, totals_in.at[z], s2_out.at[k], s2_in.at[k], along[k])
 
-    for k in range(1, nz):
+    for k in range(nz - 1, 0, -1):
         when(give_after(k), lambda k=k: total_copy(k).start())
-    when(outer, lambda: first_start((0, 1)))
     own[2].wait()
-    when(jnp.logical_not(outer), lambda: first_start((0, 3), (0, 2), (1, 1), (1, 3), (1, 2)))
-    spread(0, 1)
+    when(jnp.logical_not(outer), lambda: first_start((0, 2), (1, 1), (1, 3), (1, 2)))
+    loads[3].wait()
+
+    def gate_step(head, carry):
+        lanes = by_head(head)
+        gates[:, lanes] = silu(og_v[:, lanes].astype(jnp.float32)) * hgain_ref[...].astype(jnp.float32)
+        return carry
+
+    lax.fori_loop(0, heads, gate_step, 0)
     entry[...] = jnp.zeros_like(entry)
     for k in range(1, nz):
         when(jnp.logical_not(give_after(k)), lambda k=k: total_copy(k).wait_recv())
@@ -663,8 +671,8 @@
         factor, state = unpack(held[origin])
         entry[...] = factor * entry[...] + state
     enter[c, q] = made[q]
+    when(outer, lambda: first_start((0, 2)))
     onward(0, 1)
-    when(outer, lambda: first_start((1, 2), (1, 3), (1, 1)))
     last(0, 0)
     spread(0, 2)
     for w in range(PLANE):
@@ -672,10 +680,12 @@
         factor, state = unpack(states[c, w])
         beside[w] = (factor * enter[c, w].astype(jnp.float32) + state).astype(jnp.bfloat16)
         beside_copy(w).start()
-    for load in loads[3:]:
+    for load in loads[4:]:
         load.wait()
     for w in range(PLANE):
         beside_arrival(w).wait_recv()
+
+    when(outer, lambda: first_start((1, 2), (1, 3), (1, 1)))
 
     def mix_step(head, carry):
         lanes = by_head(head)
@@ -686,11 +696,10 @@
             + dot_nt(reach[1, :, lanes], enter[1, group, i])
         )
         scale = lax.rsqrt(jnp.mean(mix * mix, axis=-1, keepdims=True) + NORM_EPS)
-        gate = silu(og_v[:, lanes].astype(jnp.float32))
-        mixed[:, lanes] = (mix * scale * hgain_ref[...].astype(jnp.float32) * gate).astype(jnp.bfloat16)
+        mixed[:, lanes] = (mix * scale * gates[:, lanes]).astype(jnp.bfloat16)
         return carry
 
-    lax.fori_loop(0, heads, mix_step, 0)
+    lax.fori_loop(0, heads, mix_step, 0, unroll=4)
     chunk = columns // nz
 
     def hidden_step(i, carry):
@@ -808,63 +817,72 @@
 
     spread(0, 3)
     onward(0, 2)
+    last(0, 1)
+    onward(0, 3)
     spread(1, 0)
-    last(0, 1)
+    spread(1, 1)
     relay(1, 0)
-    onward(0, 3)
-    spread(1, 1)
     last(0, 2)
     settle(0, 0)
     settle(0, 1)
-    relay(1, 1)
+    last(0, 3)
     onward(1, 0)
     spread(1, 2)
-    last(0, 3)
-    relay(2, 0)
+    relay(1, 1)
     settle(0, 2)
     settle(0, 3)
-    work(0, 1, expand)
+    work(1, 2, expand)
     onward(1, 1)
     spread(1, 3)
-    work(1, 2, expand)
+    relay(2, 0)
+    last(1, 0)
+    settle(1, 0)
+    work(1, 2, lambda zz: lower(zz, 0))
+    ends(0, 1)
     relay(2, 1)
-    last(1, 0)
     work(2, 3, expand)
-    settle(1, 0)
-    work(0, 3, lambda zz: lower(zz, 0))
-    ends(0, 1, 2)
+    work(2, 3, lambda zz: lower(zz, 0))
+    ends(0, 2)
     onward(1, 2)
     last(1, 1)
     settle(1, 1)
-    work(0, 3, lambda zz: lower(zz, 1))
-    ends(1, 1, 2)
-    near_pass(0)
+    work(1, 3, lambda zz: lower(zz, 1))
+    ends(1, 2, 1)
     onward(1, 3)
     last(1, 2)
     settle(1, 2)
-    work(0, 3, lambda zz: lower(zz, 2))
-    ends(2, 1, 2)
-    near_pass(1)
+    near_pass(0)
     relay(3, 0)
     relay(3, 1)
     work(3, 4, expand)
     for s in range(3):
         work(3, 4, lambda zz, s=s: lower(zz, s))
         ends(s, 3)
+    work(1, 3, lambda zz: lower(zz, 2))
+    near_pass(1)
     last(1, 3)
     settle(1, 3)
-    near_pass(2)
+    work(3, 4, lambda zz: lower(zz, 3))
+    ends(3, 3)
+    ends(2, 2, 1)
+    work(1, 3, lambda zz: lower(zz, 3))
+    ends(3, 2, 1)
     far_pass(0)
-    work(0, 4, lambda zz: lower(zz, 3))
-    ends(3, 3, 2, 1)
     far_pass(1)
     end_pass(0)
     far_pass(2)
     end_pass(1)
+    work(0, 1, expand)
+    for s in range(nz):
+        work(0, 1, lambda zz, s=s: lower(zz, s))
     far_pass(3)
+    end_pass(2)
+    near_pass(2)
+    end_pass(3)
     near_pass(3)
-    end_pass(2)
-    end_pass(3)
+
+    def result(s):
+        return pltpu.make_async_copy(mixed.at[:, lanes_of(s)], out_ref.at[:, lanes_of(s)], in_sem.at[6 + s])
 
     def finish(s):
         when(z > 0, lambda: sum_up(z, s).wait_recv())
@@ -873,11 +891,14 @@
         added = res_v[:, lanes].astype(jnp.float32) + parts[z, :, lanes].astype(jnp.float32)
         added = added + jnp.where(z > 0, terms[0, z, :, lanes].astype(jnp.float32), 0.0)
         added = added + jnp.where(z < nz - 1, terms[1, z, :, lanes].astype(jnp.float32), 0.0)
-        out_ref[:, lanes] = added.astype(jnp.bfloat16)
+        mixed[:, lanes] = added.astype(jnp.bfloat16)
+        result(s).start()
 
     for s in range(nz):
         finish(s)
 
+    for s in range(nz):
+        result(s).wait()
     def sent(src, sem, got_sem, there):
         copy(src, src, sem, got_sem, there).wait_send()
 
@@ -925,7 +946,7 @@
     return pl.pallas_call(
         functools.partial(layer_kernel, nz),
         in_specs=[anywhere] * 5 + [near] * 4 + [anywhere] * 4,
-        out_specs=near,
+        out_specs=anywhere,
         out_shape=jax.ShapeDtypeStruct((rows, columns), bf16),
         scratch_shapes=[
             pltpu.VMEM((rows, columns), bf16),
@@ -937,6 +958,7 @@
             pltpu.VMEM((3, n * depth, units), bf16),
             pltpu.VMEM((2, rows, columns), bf16),
             pltpu.VMEM((2, rows, columns), bf16),
+            pltpu.VMEM((rows, columns), f32),
             pltpu.VMEM((rows, columns), f32),
             pltpu.VMEM((2, PLANE, per, padded, width), bf16),
             pltpu.VMEM((PLANE, per, padded, width), bf16),
@@ -953,7 +975,7 @@
             pltpu.VMEM((nz, rows, units), bf16),
             pltpu.VMEM((nz, rows, columns), bf16),
             pltpu.VMEM((2, nz, rows, columns), bf16),
-            dma((6,)),
+            dma((6 + nz,)),
             dma((3,)),
             *one_out(3, nz),
             *one_out(2, nz),

time: 143 us -> 135 us (0.944)
  the two profiles are of different devices: /device:TPU:4 before, /device:TPU:8 now
where the time goes in v3:
time: 135 us
  Pallas kernels  133 us (99%)
  local copies, waits for them, and re-layouts  1.88 us (1%)
    pallas_call x1, Pallas kernels, layer(): pl.pallas_call(functools.partial(layer_kernel, nz), in_specs=[anywhere] *...  133 us

profile of v3, /device:TPU:8, one launch (start us, length us, event | category | flops | bytes accessed | tf_op | source)
XLA Modules:
  0.0 134.6 jit_solution(3258081764880227121)
XLA Ops:
  0.0 132.7 %layer.1 = bf16[128,2048]{1,0:T(8,128)(2,1)} custom-call(bf16[128,2048]{1,0:T(8,128)(2,1)} %q_hbm.1, bf16[2,128,2048]{2,1,0:T(8,128)(2,1)} %f_hbm.1, bf16[128,2048]{1,0:T(8,128)(2,1)} %v_hbm.1, bf16[128,2048]{1,0:T(8,128)(2,1)} %og_hbm.1, bf16[128,2048]{1,0:T(8,128)(2,1)} %res_hbm.1, f32[1,2048]{1,0:T(1,128)} %bitcast.6, f32[16,128]{1,0:T(8,128)} %bitcast.7, ...), custom_call_target="tpu_custom_call" | custom-call | tf_op jit(solution)/shard_map/layer/pallas_call | solution.py:946
  132.8 1.9 %copy.15 = bf16[128,2048]{1,0:T(8,128)(2,1)} copy(bf16[128,2048]{1,0:T(8,128)(2,1)} %layer.1) | data formatting | bytes 1048576

commit v4 on v3

--- a/solution.py
+++ b/solution.py
@@ -474,10 +474,13 @@
         src = piece(part, k, 0)
         return copy(src, src, y_out.at[0], y_in.at[part, k], y_dev)
 
-    def corner(part, k):
-        near, there = (1, y_dev) if k < nz // 2 else (2, x_dev)
-        src = piece(part, k, near)
-        return copy(src, src, d_out.at[0], d_in.at[part, k], there)
+    def corner(part, k, j):
+        near, there = ((1, y_dev), (2, x_dev))[j]
+        row, lo, count = at(source(part, k), qs[near], c) * depth, j, depth
+        if part == 1:
+            row, lo, count = row + j * (depth // 2), 2, depth // 2
+        src = w_v.at[pl.ds(lo, 1), pl.ds(pl.multiple_of(row, count), count), :]
+        return copy(src, src, d_out.at[0], d_in.at[j, part, k], there)
 
     def partner(part, k, j):
         src = piece(part, k, j)
@@ -495,16 +498,15 @@
 
     def onward(part, k):
         across_x(part, k).wait_recv()
-        if k < nz // 2:
-            corner(part, k).start()
+        corner(part, k, 0).start()
         partner(part, k, 1).start()
         across_y(part, k).wait_recv()
-        if k >= nz // 2:
-            corner(part, k).start()
+        corner(part, k, 1).start()
         partner(part, k, 2).start()
 
     def last(part, k):
-        corner(part, k).wait_recv()
+        corner(part, k, 0).wait_recv()
+        corner(part, k, 1).wait_recv()
         partner(part, k, 3).start()
 
     def settle(part, k):
@@ -905,7 +907,7 @@
     sent(w_v.at[:, 0 : (nz - 1) * depth], w1_out.at[0], w1_in.at[0, 0], x_dev)
     sent(w_v.at[:, 0 : nz * depth], x_out.at[0], x_in.at[0, 0], x_dev)
     sent(w_v.at[:, 0 : nz * depth], y_out.at[0], y_in.at[0, 0], y_dev)
-    sent(w_v.at[:, 0 : nz * depth], d_out.at[0], d_in.at[0, 0], x_dev)
+    sent(w_v.at[:, 0 : nz * depth], d_out.at[0], d_in.at[0, 0, 0], x_dev)
     sent(w_v.at[:, 0 : PLANE * nz * depth], p_out.at[0], p_in.at[0, 0, 0], p_dev)
     sent(parts.at[0 : nz - 1], r_out.at[0], r_in.at[0, 0, 0], x_dev)
     for k in range(1, nz):
@@ -980,7 +982,7 @@
             *one_out(3, nz),
             *one_out(2, nz),
             *one_out(2, nz),
-            *one_out(2, nz),
+            *one_out(2, 2, nz),
             *one_out(2, nz, PLANE),
             *pairs(PLANE),
             *pairs(PLANE),

time: 135 us -> 125 us (0.926)
  Pallas kernels: 133 us -> 122 us
    pallas_call x1, Pallas kernels: 133 us -> 122 us  [layer(): pl.pallas_call(functools.partial(layer_kernel, nz), in_specs=[anywhere] *...]
where the time goes in v4:
time: 125 us; the launch traced here: 124 us
  Pallas kernels  122 us (98%)
  local copies, waits for them, and re-layouts  1.88 us (2%)
    pallas_call x1, Pallas kernels, layer(): pl.pallas_call(functools.partial(layer_kernel, nz), in_specs=[anywhere] *...  122 us

profile of v4, /device:TPU:8, one launch (start us, length us, event | category | flops | bytes accessed | tf_op | source)
XLA Modules:
  0.0 124.2 jit_solution(6241048814072874652)
XLA Ops:
  0.0 122.3 %layer.1 = bf16[128,2048]{1,0:T(8,128)(2,1)} custom-call(bf16[128,2048]{1,0:T(8,128)(2,1)} %q_hbm.1, bf16[2,128,2048]{2,1,0:T(8,128)(2,1)} %f_hbm.1, bf16[128,2048]{1,0:T(8,128)(2,1)} %v_hbm.1, bf16[128,2048]{1,0:T(8,128)(2,1)} %og_hbm.1, bf16[128,2048]{1,0:T(8,128)(2,1)} %res_hbm.1, f32[1,2048]{1,0:T(1,128)} %bitcast.6, f32[16,128]{1,0:T(8,128)} %bitcast.7, ...), custom_call_target="tpu_custom_call" | custom-call | tf_op jit(solution)/shard_map/layer/pallas_call | solution.py:948
  122.3 1.9 %copy.15 = bf16[128,2048]{1,0:T(8,128)(2,1)} copy(bf16[128,2048]{1,0:T(8,128)(2,1)} %layer.1) | data formatting | bytes 1048576
